TPU v7x, 512 devices: a whole 4x8x8 slice. The times are simulated.
512 devices in a mesh: ep: 32 (over z, x), tp: 16 (over y, core).
Axes of the slice: x: 4, y: 8, z: 8, core: 2. Of those that a mesh axis runs over, the one named last changes fastest.
Arguments:
- tokens: bfloat16 [256, 4096], P('ep', 'tp'), may hold values from -6 to 6
- norm_gain: float32 [4096], replicated, may hold values from 0.1 to 1.9
- route_experts: int32 [256, 2], P('ep'), may hold values from 0 to 63, all different within a row; in each aligned block of 8 rows (0 to 7, 8 to 15, ...) at most 2 rows name the same one
- route_logits: float32 [256, 2], P('ep'), may hold values from -4 to 4
- expert_gate: bfloat16 [64, 4096, 1024], P('ep', None, 'tp'), may hold values from -0.09375 to 0.09375
- expert_up: bfloat16 [64, 4096, 1024], P('ep', None, 'tp'), may hold values from -0.09375 to 0.09375
- expert_down: bfloat16 [64, 1024, 4096], P('ep', 'tp'), may hold values from -0.1875 to 0.1875
- dense_gate: bfloat16 [4096, 1024], P(None, 'tp'), may hold values from -0.09375 to 0.09375
- dense_up: bfloat16 [4096, 1024], P(None, 'tp'), may hold values from -0.09375 to 0.09375
- dense_down: bfloat16 [1024, 4096], P('tp'), may hold values from -0.1875 to 0.1875
- mix_weight: float32 [4096], replicated, may hold values from -0.09375 to 0.09375
- out_gain: float32 [4096], P('tp'), may hold values from 0.1 to 1.9
Outputs:
- result: bfloat16 [256, 4096], P('ep', 'tp')
Inputs may be any that keep to these rules, and one draw needn't show every extreme that they name: `route_experts`: each row names 2 different experts; the 8 rows of one index of ep (aligned blocks) name any one expert at most 2 times, and some block names some expert exactly 2 times; every expert is named somewhere.
All inputs are finite; a program needn't handle non-finite values.
Results may differ from a plain program's by a relative error of at most 0.0025.
Values may be sent and summed in bfloat16 or wider, within the bound.
A program may use at most 64 MiB of HBM per device.

v0:
```python
import jax
import jax.numpy as jnp
from jax import lax
from jax.sharding import Mesh
from jax.sharding import PartitionSpec as P

CAP = 2
TP = ("tp_0", "tp_1")
norm_eps = 1e-06


def summed_rows(x, axes, dim):
    if not axes:
        return x
    nearer = lax.psum_scatter(x, axes[0], scatter_dimension=dim, tiled=True)
    return summed_rows(nearer, axes[1:], dim)


def local(
    tokens,
    norm_gain,
    route_experts,
    route_logits,
    expert_gate,
    expert_up,
    expert_down,
    dense_gate,
    dense_up,
    dense_down,
    mix_weight,
    out_gain,
):
    tok_rows, width_part = tokens.shape
    groups = lax.axis_size(TP)
    width = width_part * groups
    whole_rows = lax.all_gather(tokens, TP, axis=1, tiled=True).astype(jnp.float32)
    normed = (
        whole_rows
        * lax.rsqrt(jnp.mean(whole_rows * whole_rows, axis=1, keepdims=True) + norm_eps)
        * norm_gain
    ).astype(jnp.bfloat16)
    weights = jax.nn.softmax(route_logits, axis=-1)
    top_count = route_experts.shape[1]
    local_experts = expert_gate.shape[0]
    peer_count = lax.axis_size("ep")
    experts = local_experts * peer_count
    dense_hidden = (
        jax.nn.silu(jnp.dot(normed, dense_gate, preferred_element_type=jnp.float32))
        * jnp.dot(normed, dense_up, preferred_element_type=jnp.float32)
    ).astype(jnp.bfloat16)
    dense_out = summed_rows(
        jnp.dot(dense_hidden, dense_down, preferred_element_type=jnp.float32), TP, 1
    )
    mix_gate = jax.nn.sigmoid(
        jnp.dot(normed.astype(jnp.float32), mix_weight, precision=lax.Precision.HIGHEST)
    )
    flat_routes = route_experts.reshape(-1)
    expert_ids = jnp.arange(experts, dtype=jnp.int32)
    capacity = CAP
    slot_count = experts * capacity
    route_hits = (flat_routes[:, None] == expert_ids[None, :]).astype(jnp.int32)
    before = jnp.cumsum(route_hits, axis=0) - route_hits
    slot_rank = jnp.sum(before * route_hits, axis=1)
    position = flat_routes * capacity + slot_rank
    onehot_place = (position[:, None] == jnp.arange(slot_count, dtype=jnp.int32)[None, :]).astype(
        jnp.float32
    )
    placing = jnp.sum(onehot_place.reshape(tok_rows, top_count, slot_count), axis=1).T.astype(
        jnp.bfloat16
    )
    outgoing = jnp.dot(placing, normed, preferred_element_type=jnp.float32).astype(jnp.bfloat16)
    received = lax.all_to_all(outgoing, "ep", split_axis=0, concat_axis=0, tiled=True)
    arranged = (
        received.reshape(peer_count, local_experts, capacity, width)
        .transpose(1, 0, 2, 3)
        .reshape(local_experts, peer_count * capacity, width)
    )
    gate_act = jnp.einsum("erd,edf->erf", arranged, expert_gate, preferred_element_type=jnp.float32)
    up_act = jnp.einsum("erd,edf->erf", arranged, expert_up, preferred_element_type=jnp.float32)
    hidden = (jax.nn.silu(gate_act) * up_act).astype(jnp.bfloat16)
    partial_value = jnp.einsum(
        "erf,efd->erd", hidden, expert_down, preferred_element_type=jnp.float32
    )
    summed = lax.psum_scatter(partial_value, TP, scatter_dimension=2, tiled=True)
    back_send = (
        summed.reshape(local_experts, peer_count, capacity, width_part)
        .transpose(1, 0, 2, 3)
        .reshape(slot_count, width_part)
    )
    returned = lax.all_to_all(back_send, "ep", split_axis=0, concat_axis=0, tiled=True)
    combine_map = jnp.sum(
        (onehot_place * weights.reshape(-1)[:, None]).reshape(tok_rows, top_count, slot_count),
        axis=1,
    )
    expert_mix = jnp.dot(combine_map, returned, precision=lax.Precision.HIGHEST)
    combined = expert_mix + mix_gate[:, None] * dense_out
    squares_out = lax.psum(jnp.sum(combined * combined, axis=1), TP)
    result = combined * lax.rsqrt(squares_out[:, None] / width + norm_eps) * out_gain
    return result.astype(jnp.bfloat16)


def solution(mesh):
    split = Mesh(mesh.devices.reshape(mesh.shape["ep"], 8, 2), ("ep", "tp_0", "tp_1"))
    in_specs = (
        P("ep", TP),
        P(),
        P("ep", None),
        P("ep", None),
        P("ep", None, TP),
        P("ep", None, TP),
        P("ep", TP, None),
        P(None, TP),
        P(None, TP),
        P(TP, None),
        P(),
        P(TP),
    )
    out_specs = P("ep", TP)
    return jax.shard_map(local, mesh=split, in_specs=in_specs, out_specs=out_specs, check_vma=False)
```

profile of v0, /device:TPU:2, one launch (start us, length us, event | category | flops | bytes accessed | tf_op | source)
XLA Modules:
  0.0 229.2 jit_solution(5264460515615627035)
XLA Ops:
  6.5 0.8 reduce_max.9
  7.3 0.7 fusion.26
  8.0 0.7 fusion.25
  8.7 0.8 copy.34
  10.0 18.0 %all_gather.3 = bf16[8,4096]{1,0:T(8,128)(2,1)S(1)} all-gather(bf16[8,256]{1,0:T(8,128)(2,1)} %param.12), channel_id=1, replica_groups=mesh['ep'=32,'tp_0'=8,'tp_1'=2] {'tp_0','tp_1'}, dimensions={1}, use_global_device_ids=true | all-gather | bytes 69632 | tf_op jit(solution)/shard_map/all_gather | solution.py:36
  28.2 1.2 convolution_convert_fusion
  29.5 0.4 all_to_all.14
  29.9 41.8 %all_to_all.21 = bf16[32,4,4096]{2,1,0:T(4,128)(2,1)S(1)} all-to-all(bf16[32,4,4096]{2,1,0:T(4,128)(2,1)S(1)} %all_to_all.14), channel_id=1, replica_groups=mesh['ep'=32,'tp_0'=8,'tp_1'=2] {'ep'}, dimensions={0} | all-to-all | bytes 2097152 | tf_op jit(solution)/shard_map/all_to_all | solution.py:72
  71.7 0.5 reshape.67
  72.3 2.0 copy.41
  74.3 1.6 reshape.68
  75.9 0.4 fusion.35
  76.3 3.4 %fusion.1 = f32[2,64,4096]{2,1,0:T(8,128)} fusion(bf16[2,64,4096]{2,1,0:T(8,128)(2,1)S(1)} %copy-done, bf16[2,64,4096]{2,1,0:T(8,128)(2,1)S(1)} %reshape.68, bf16[2,4096,64]{1,2,0:T(8,128)(2,1)} %param.17, f32[2,64,64]{2,1,0:T(8,128)S(1)} %fusion.35), kind=kOutput, calls=%fused_computation.3 | convolution fusion | flops 134266880 | bytes 5275648 | tf_op jit(solution)/shard_map/erf,efd->erd/dot_general | solution.py:81
  79.8 0.9 copy-done.2
  81.1 1.3 fusion.3
  82.4 53.8 %reduce-scatter.4.cloned.1.call-done = f32[2,64,256]{2,1,0:T(8,128)} async-done(((f32[2,64,4096]{2,1,0:T(8,128)}), f32[2,64,256]{2,1,0:T(8,128)}) %reduce-scatter.4.cloned.1.call-update) | async-done | bytes 131088 | tf_op jit(solution)/shard_map/reduce_scatter | solution.py:84
  136.1 1.0 reshape.69
  137.1 0.7 copy.39
  137.8 10.5 %all-to-all-start.1 = ((f32[32,4,256]{2,1,0:T(4,128)}), f32[32,4,256]{2,1,0:T(4,128)S(1)}, u32[]{:S(2)}, u32[]{:S(2)}) async-start(f32[32,4,256]{2,1,0:T(4,128)} %copy.39), calls=%async_computation.2 | async-start | bytes 262144 | tf_op jit(solution)/shard_map/all_to_all | solution.py:90
  148.4 28.9 %reduce-scatter.6.cloned.1.call-done = f32[8,512]{1,0:T(8,128)} async-done(((f32[8,4096]{1,0:T(8,128)}), f32[8,512]{1,0:T(8,128)}) %reduce-scatter.6.cloned.1.call-update) | async-done | bytes 16400 | tf_op jit(solution)/shard_map/reduce_scatter | solution.py:15
  177.7 16.9 %reduce-scatter.8.cloned.1.call-done = f32[8,256]{1,0:T(8,128)} async-done(((f32[8,512]{1,0:T(8,128)}), f32[8,256]{1,0:T(8,128)}) %reduce-scatter.8.cloned.1.call-update) | async-done | bytes 8208 | tf_op jit(solution)/shard_map/reduce_scatter | solution.py:15
  194.6 1.0 multiply_reduce_fusion
  195.6 26.3 %psum.7 = f32[8]{0:T(128)S(1)} all-reduce(f32[8]{0:T(128)S(1)} %get-tuple-element.7), channel_id=1, replica_groups=mesh['ep'=32,'tp_0'=8,'tp_1'=2] {'tp_0','tp_1'}, use_global_device_ids=true, to_apply=%region_11.12 | all-reduce | flops 8 | bytes 64 | tf_op jit(solution)/shard_map/psum | solution.py:97
  222.0 0.7 multiply_convert_fusion
  (37 shorter events, 1.7 us)
Async XLA Ops:
  6.5 69.8 %copy-start = (bf16[2,64,4096]{2,1,0:T(8,128)(2,1)S(1)}, bf16[2,64,4096]{2,1,0:T(8,128)(2,1)}, u32[]{:S(2)}) copy-start(bf16[2,64,4096]{2,1,0:T(8,128)(2,1)} %param.18) | copy-start | bytes 3145732
  6.5 129.6 %reduce-scatter.4.cloned.1.call-start = ((), (), s32[]{:S(2)}) async-start(), calls=%async_computation.5 | async-start | bytes 2228224 | tf_op jit(solution)/shard_map/reduce_scatter | solution.py:84
  74.3 1.6 copy-start.1
  79.7 1.0 copy-start.2
  79.7 1.0 copy-start.5
  79.7 1.3 copy-start.3
  79.7 1.4 copy-start.4
  79.7 97.6 %copy-start.7 = (f32[4096]{0:T(1024)S(1)}, f32[4096]{0:T(1024)}, u32[]{:S(2)}) copy-start(f32[4096]{0:T(1024)} %param.22) | copy-start | bytes 49156
  79.7 142.2 %copy-start.6 = (f32[256]{0:T(256)S(1)}, f32[256]{0:T(256)}, u32[]{:S(2)}) copy-start(f32[256]{0:T(256)} %param.23) | copy-start | bytes 3076
  79.8 97.6 %reduce-scatter.6.cloned.1.call-start = ((), (), s32[]{:S(2)}) async-start(), calls=%async_computation.6 | async-start | bytes 147456 | tf_op jit(solution)/shard_map/reduce_scatter | solution.py:15
  137.8 39.8 %all-to-all-start.1 = ((f32[32,4,256]{2,1,0:T(4,128)}), f32[32,4,256]{2,1,0:T(4,128)S(1)}, u32[]{:S(2)}, u32[]{:S(2)}) async-start(f32[32,4,256]{2,1,0:T(4,128)} %copy.39), calls=%async_computation.2 | async-start | bytes 262144 | tf_op jit(solution)/shard_map/all_to_all | solution.py:90
  148.3 46.3 %reduce-scatter.8.cloned.1.call-start = ((), (), s32[]{:S(2)}) async-start(), calls=%async_computation.7 | async-start | bytes 24576 | tf_op jit(solution)/shard_map/reduce_scatter | solution.py:15
Sparse Core Ops, SparseCore 0:
  79.9 56.2 reduce-scatter.3
  138.9 38.3 reduce-scatter.5
  180.0 14.5 reduce-scatter.7
where the time goes:
time: 230 us; the launch traced here: 229 us
  waiting for transfers between devices  99.7 us (43%)
  blocking collectives  86.2 us (37%)
  between operations  13.2 us (6%)
  starting transfers between devices  10.6 us (5%)
  local copies, waits for them, and re-layouts  8.3 us (4%)
  matrix products  7.8 us (3%)
  other arithmetic  3.38 us (1%)
    reduce_scatter x1, waiting for transfers between devices, local(): lax.psum_scatter(partial_value, TP, scatter_dimension=2, tiled=True)  53.8 us
    reduce_scatter x2, waiting for transfers between devices, summed_rows(): nearer = lax.psum_scatter(x, axes[0], scatter_dimension=dim, tiled=True)  45.8 us
    all_to_all x1, blocking collectives, local(): lax.all_to_all(outgoing, 'ep', split_axis=0, concat_axis=0, tiled=True)  41.8 us
    psum x1, blocking collectives, local(): squares_out = lax.psum(jnp.sum(combined * combined, axis=1), TP)  26.3 us
    all_gather x1, blocking collectives, local(): lax.all_gather(tokens, TP, axis=1, tiled=True).astype(jnp.float32)  18 us
    all_to_all x1, starting transfers between devices, local(): lax.all_to_all(back_send, 'ep', split_axis=0, concat_axis=0, tiled=True)  10.5 us
  transfers between devices with their start and end apart: 4, of which 3 were waited for; matrix products, arithmetic and copies ran while one was open for 2% of the time, Pallas kernels for 0%

commit v1 on v0

--- a/solution.py
+++ b/solution.py
@@ -94,7 +94,7 @@
     )
     expert_mix = jnp.dot(combine_map, returned, precision=lax.Precision.HIGHEST)
     combined = expert_mix + mix_gate[:, None] * dense_out
-    squares_out = lax.psum(jnp.sum(combined * combined, axis=1), TP)
+    squares_out = lax.psum(lax.psum(jnp.sum(combined * combined, axis=1), "tp_1"), "tp_0")
     result = combined * lax.rsqrt(squares_out[:, None] / width + norm_eps) * out_gain
     return result.astype(jnp.bfloat16)
 

time: 230 us -> 223 us (0.970)
  blocking collectives: 86.2 us -> 79.3 us
    psum x1 -> x2, blocking collectives: 26.3 us -> 19.5 us  [the longest x1 17 us: local(): lax.psum(lax.psum(jnp.sum(combined * combined, axis=1), 'tp_1'), 'tp_0')]
where the time goes in v1:
time: 223 us; the launch traced here: 222 us
  waiting for transfers between devices  99.7 us (45%)
  blocking collectives  79.3 us (36%)
  between operations  13.2 us (6%)
  starting transfers between devices  10.6 us (5%)
  local copies, waits for them, and re-layouts  8.3 us (4%)
  matrix products  7.8 us (3%)
  other arithmetic  3.38 us (2%)
    reduce_scatter x1, waiting for transfers between devices, local(): lax.psum_scatter(partial_value, TP, scatter_dimension=2, tiled=True)  53.8 us
    reduce_scatter x2, waiting for transfers between devices, summed_rows(): nearer = lax.psum_scatter(x, axes[0], scatter_dimension=dim, tiled=True)  45.8 us
    all_to_all x1, blocking collectives, local(): lax.all_to_all(outgoing, 'ep', split_axis=0, concat_axis=0, tiled=True)  41.8 us
    all_gather x1, blocking collectives, local(): lax.all_gather(tokens, TP, axis=1, tiled=True).astype(jnp.float32)  18 us
    psum x1, blocking collectives, local(): lax.psum(lax.psum(jnp.sum(combined * combined, axis=1), 'tp_1'), 'tp_0')  17 us
    all_to_all x1, starting transfers between devices, local(): lax.all_to_all(back_send, 'ep', split_axis=0, concat_axis=0, tiled=True)  10.5 us
  transfers between devices with their start and end apart: 4, of which 3 were waited for; matrix products, arithmetic and copies ran while one was open for 2% of the time, Pallas kernels for 0%

profile of v1, /device:TPU:2, one launch (start us, length us, event | category | flops | bytes accessed | tf_op | source)
XLA Modules:
  0.0 222.3 jit_solution(1609646129384233663)
XLA Ops:
  6.5 0.8 reduce_max.9
  7.3 0.7 fusion.26
  8.0 0.7 fusion.25
  8.7 0.8 copy.34
  10.0 18.0 %all_gather.3 = bf16[8,4096]{1,0:T(8,128)(2,1)S(1)} all-gather(bf16[8,256]{1,0:T(8,128)(2,1)} %param.12), channel_id=1, replica_groups=mesh['ep'=32,'tp_0'=8,'tp_1'=2] {'tp_0','tp_1'}, dimensions={1}, use_global_device_ids=true | all-gather | bytes 69632 | tf_op jit(solution)/shard_map/all_gather | solution.py:36
  28.2 1.2 convolution_convert_fusion
  29.5 0.4 all_to_all.14
  29.9 41.8 %all_to_all.21 = bf16[32,4,4096]{2,1,0:T(4,128)(2,1)S(1)} all-to-all(bf16[32,4,4096]{2,1,0:T(4,128)(2,1)S(1)} %all_to_all.14), channel_id=1, replica_groups=mesh['ep'=32,'tp_0'=8,'tp_1'=2] {'ep'}, dimensions={0} | all-to-all | bytes 2097152 | tf_op jit(solution)/shard_map/all_to_all | solution.py:72
  71.7 0.5 reshape.67
  72.3 2.0 copy.41
  74.3 1.6 reshape.68
  76.3 3.4 %fusion.1 = f32[2,64,4096]{2,1,0:T(8,128)} fusion(bf16[2,64,4096]{2,1,0:T(8,128)(2,1)S(1)} %copy-done, bf16[2,64,4096]{2,1,0:T(8,128)(2,1)S(1)} %reshape.68, bf16[2,4096,64]{1,2,0:T(8,128)(2,1)} %param.17, f32[2,64,64]{2,1,0:T(8,128)S(1)} %fusion.35), kind=kOutput, calls=%fused_computation.3 | convolution fusion | flops 134266880 | bytes 5275648 | tf_op jit(solution)/shard_map/erf,efd->erd/dot_general | solution.py:81
  79.8 0.9 copy-done.2
  81.1 1.3 fusion.3
  82.4 53.8 %reduce-scatter.4.cloned.1.call-done = f32[2,64,256]{2,1,0:T(8,128)} async-done(((f32[2,64,4096]{2,1,0:T(8,128)}), f32[2,64,256]{2,1,0:T(8,128)}) %reduce-scatter.4.cloned.1.call-update) | async-done | bytes 131088 | tf_op jit(solution)/shard_map/reduce_scatter | solution.py:84
  136.1 1.0 reshape.69
  137.1 0.7 copy.39
  137.8 10.5 %all-to-all-start.1 = ((f32[32,4,256]{2,1,0:T(4,128)}), f32[32,4,256]{2,1,0:T(4,128)S(1)}, u32[]{:S(2)}, u32[]{:S(2)}) async-start(f32[32,4,256]{2,1,0:T(4,128)} %copy.39), calls=%async_computation.2 | async-start | bytes 262144 | tf_op jit(solution)/shard_map/all_to_all | solution.py:90
  148.4 28.9 %reduce-scatter.6.cloned.1.call-done = f32[8,512]{1,0:T(8,128)} async-done(((f32[8,4096]{1,0:T(8,128)}), f32[8,512]{1,0:T(8,128)}) %reduce-scatter.6.cloned.1.call-update) | async-done | bytes 16400 | tf_op jit(solution)/shard_map/reduce_scatter | solution.py:15
  177.7 16.9 %reduce-scatter.8.cloned.1.call-done = f32[8,256]{1,0:T(8,128)} async-done(((f32[8,512]{1,0:T(8,128)}), f32[8,256]{1,0:T(8,128)}) %reduce-scatter.8.cloned.1.call-update) | async-done | bytes 8208 | tf_op jit(solution)/shard_map/reduce_scatter | solution.py:15
  194.6 1.0 multiply_reduce_fusion
  195.6 2.5 %psum.14 = f32[8]{0:T(128)S(1)} all-reduce(f32[8]{0:T(128)S(1)} %get-tuple-element.7), channel_id=1, replica_groups=mesh['ep'=32,'tp_0'=8,'tp_1'=2] {'tp_1'}, use_global_device_ids=true, to_apply=%region_11.12 | all-reduce | flops 8 | bytes 64 | tf_op jit(solution)/shard_map/psum | solution.py:97
  198.1 17.0 %psum.15 = f32[8]{0:T(128)S(1)} all-reduce(f32[8]{0:T(128)S(1)} %psum.14), channel_id=1, replica_groups=mesh['ep'=32,'tp_0'=8,'tp_1'=2] {'tp_0'}, use_global_device_ids=true, to_apply=%region_12.13 | all-reduce | flops 8 | bytes 64 | tf_op jit(solution)/shard_map/psum | solution.py:97
  215.1 0.7 multiply_convert_fusion
  (38 shorter events, 2.1 us)
Async XLA Ops:
  6.5 69.8 %copy-start = (bf16[2,64,4096]{2,1,0:T(8,128)(2,1)S(1)}, bf16[2,64,4096]{2,1,0:T(8,128)(2,1)}, u32[]{:S(2)}) copy-start(bf16[2,64,4096]{2,1,0:T(8,128)(2,1)} %param.18) | copy-start | bytes 3145732
  6.5 129.6 %reduce-scatter.4.cloned.1.call-start = ((), (), s32[]{:S(2)}) async-start(), calls=%async_computation.5 | async-start | bytes 2228224 | tf_op jit(solution)/shard_map/reduce_scatter | solution.py:84
  74.3 1.6 copy-start.1
  79.7 1.0 copy-start.2
  79.7 1.0 copy-start.5
  79.7 1.3 copy-start.3
  79.7 1.4 copy-start.4
  79.7 97.6 %copy-start.7 = (f32[4096]{0:T(1024)S(1)}, f32[4096]{0:T(1024)}, u32[]{:S(2)}) copy-start(f32[4096]{0:T(1024)} %param.22) | copy-start | bytes 49156
  79.7 135.3 %copy-start.6 = (f32[256]{0:T(256)S(1)}, f32[256]{0:T(256)}, u32[]{:S(2)}) copy-start(f32[256]{0:T(256)} %param.23) | copy-start | bytes 3076
  79.8 97.6 %reduce-scatter.6.cloned.1.call-start = ((), (), s32[]{:S(2)}) async-start(), calls=%async_computation.6 | async-start | bytes 147456 | tf_op jit(solution)/shard_map/reduce_scatter | solution.py:15
  137.8 39.8 %all-to-all-start.1 = ((f32[32,4,256]{2,1,0:T(4,128)}), f32[32,4,256]{2,1,0:T(4,128)S(1)}, u32[]{:S(2)}, u32[]{:S(2)}) async-start(f32[32,4,256]{2,1,0:T(4,128)} %copy.39), calls=%async_computation.2 | async-start | bytes 262144 | tf_op jit(solution)/shard_map/all_to_all | solution.py:90
  148.3 46.3 %reduce-scatter.8.cloned.1.call-start = ((), (), s32[]{:S(2)}) async-start(), calls=%async_computation.7 | async-start | bytes 24576 | tf_op jit(solution)/shard_map/reduce_scatter | solution.py:15
Sparse Core Ops, SparseCore 0:
  79.9 56.2 reduce-scatter.3
  138.9 38.3 reduce-scatter.5
  180.0 14.5 reduce-scatter.7
